TPU v7x, 512 devices: a whole 4x8x8 slice. The times are simulated.
512 devices in a mesh: sp: 32 (over z, x), tp: 16 (over y, core).
Axes of the slice: x: 4, y: 8, z: 8, core: 2. Of those that a mesh axis runs over, the one named last changes fastest.
Arguments:
- cotangent: bfloat16 [4096, 2048], P('sp'), may hold values from -6 to 6
- mixer_out: bfloat16 [4096, 2048], P('sp'), may hold values from -6 to 6
- expert_ids: int32 [4096, 2], P('sp'), may hold values from 0 to 31, all different within a row; in each aligned block of 128 rows (0 to 127, 128 to 255, ...) at most 16 rows name the same one
- route_weight: float32 [4096, 2], P('sp'), may hold values from 0.3 to 1.5
- saved_normalized: bfloat16 [4096, 2048], P('sp', 'tp'), may hold values from -6 to 6
- inverse_deviation: float32 [4096], P('sp'), may hold values from 0.3 to 3
- channel_norm_gain: float32 [2048], P('tp'), may hold values from 0.1 to 1.9
- taps: float32 [31, 2048], P(None, 'tp'), may hold values from -1 to 1
- proj_weight: bfloat16 [2048, 2048], P('tp'), may hold values from -0.125 to 0.125
- gate_weight: bfloat16 [32, 2048, 2048], P('sp', None, 'tp'), may hold values from -0.125 to 0.125
- up_weight: bfloat16 [32, 2048, 2048], P('sp', None, 'tp'), may hold values from -0.125 to 0.125
- down_weight: bfloat16 [32, 2048, 2048], P('sp', 'tp'), may hold values from -0.125 to 0.125
Outputs:
- grad_mixer_in: bfloat16 [4096, 2048], P('sp', 'tp')
- grad_proj: float32 [2048, 2048], P('sp', 'tp')
- grad_gate: bfloat16 [32, 2048, 2048], P('sp', None, 'tp')
- grad_up: bfloat16 [32, 2048, 2048], P('sp', None, 'tp')
- grad_down: bfloat16 [32, 2048, 2048], P('sp', 'tp')
Inputs may be any that keep to these rules, and one draw needn't show every extreme that they name: `expert_ids`: each row names 2 different experts. Within the rows of one index of sp no expert is named more than 16 times, a bound that some block reaches.
All inputs are finite; a program needn't handle non-finite values.
Results may differ from a plain program's by a relative error of at most 0.02.
Values may be sent and summed in bfloat16 or wider, within the bound.
No kernel may reach another device: no remote copies, remote signals or barrier semaphores. Data moves between devices by JAX's collectives and lax.ppermute only.
A program may use at most 64 MiB of HBM per device.

v0:
```python
import jax
import jax.numpy as jnp
from jax import lax
from jax.sharding import PartitionSpec as P


def sent_together(arrays, axis, split_dim, concat_dim, along):
    both = jnp.concatenate(arrays, axis=along)
    filled, at, finished = (
        lax.all_to_all(both, axis, split_axis=split_dim, concat_axis=concat_dim, tiled=True),
        0,
        [],
    )
    for a in arrays:
        finished.append(lax.slice_in_dim(filled, at, at + a.shape[along], axis=along))
        at += a.shape[along]
    return tuple(finished)


def side_by_side(arrays, axis, dim, along):
    ends, at = ([], 0)
    for a in arrays[:-1]:
        at += a.shape[along]
        ends.append(at)
    both = jnp.concatenate(arrays, axis=along)
    return tuple(jnp.split(lax.all_gather(both, axis, axis=dim, tiled=True), ends, axis=along))


def in_blocks(value, dim, size):
    dims = value.shape
    pieces = value.reshape(*dims[:dim], size, dims[dim] // size, *dims[dim + 1 :])
    return jnp.moveaxis(pieces, dim, 0)


def sent_and_summed(value, axis, dim):
    pieces = in_blocks(value, dim, lax.axis_size(axis))
    arrived = lax.all_to_all(pieces, axis, split_axis=0, concat_axis=0, tiled=True)
    return arrived.astype(jnp.float32).sum(axis=0)


def sent_to_all(value, axis):
    size = lax.axis_size(axis)
    return lax.all_to_all(
        jnp.broadcast_to(value[None], (size, *value.shape)), axis, 0, 0, tiled=True
    )


def taken_together(value, axis):
    everything = sent_to_all(value, axis)
    return jnp.sum(everything, axis=0)


def packed_total(arrays, axis):
    ends = [0]
    for a in arrays:
        ends.append(ends[-1] + a.size)
    running = taken_together(jnp.concatenate([a.ravel() for a in arrays]), axis)
    return tuple((running[b:e].reshape(a.shape) for a, b, e in zip(arrays, ends, ends[1:])))


def from_behind(value, axis, steps):
    count = lax.axis_size(axis)
    leading, last = (max(0, -steps), min(count, count - steps))
    return lax.ppermute(value, axis, [(source, source + steps) for source in range(leading, last)])


def route_table(expert_ids, route_weight, slot_start, slot_span, capacity, experts):
    onehot = (expert_ids[:, :, None] == jnp.arange(experts, dtype=jnp.int32)[None, None, :]).astype(
        jnp.int32
    )
    flat_hot = onehot.reshape(-1, experts)
    ranks = jnp.cumsum(flat_hot, axis=0) - flat_hot
    rank_pair = jnp.sum(ranks * flat_hot, axis=1).reshape(expert_ids.shape)
    slot_index = expert_ids * capacity + rank_pair
    targets = (
        jnp.arange(experts, dtype=jnp.int32)[:, None] * capacity
        + slot_start
        + jnp.arange(slot_span, dtype=jnp.int32)[None, :]
    ).reshape(-1)
    matched = slot_index[None, :, :] == targets[:, None, None]
    dispatch = jnp.any(matched, axis=2).astype(jnp.bfloat16)
    slot_weight = jnp.sum(jnp.where(matched, route_weight[None, :, :], 0.0), axis=(1, 2))
    return (dispatch, slot_weight)


def shards(
    cotangent,
    mixer_out,
    expert_ids,
    route_weight,
    saved_normalized,
    inverse_deviation,
    channel_norm_gain,
    taps,
    proj_weight,
    gate_weight,
    up_weight,
    down_weight,
):
    experts = lax.axis_size("sp")
    groups = lax.axis_size("tp")
    tok_rows, model_width = cotangent.shape
    capacity = groups * max(1, 4 * tok_rows // (experts * groups))
    slot_span = capacity // groups
    slot_start = lax.axis_index("tp") * slot_span
    dispatch, slot_weight = route_table(
        expert_ids, route_weight, slot_start, slot_span, capacity, experts
    )
    sent_rows = jnp.dot(dispatch, mixer_out, preferred_element_type=jnp.float32).astype(
        jnp.bfloat16
    )
    sent_grad = (
        slot_weight[:, None] * jnp.dot(dispatch, cotangent, preferred_element_type=jnp.float32)
    ).astype(jnp.bfloat16)
    sent_rows = sent_rows.reshape(experts, slot_span, model_width)
    sent_grad = sent_grad.reshape(experts, slot_span, model_width)
    shared_rows = sent_together((sent_rows, sent_grad), "sp", 0, 0, 1)
    routed_rows, routed_grad = side_by_side((shared_rows[0], shared_rows[1]), "tp", 1, 0)
    full_table, unused_weight = route_table(
        expert_ids, route_weight, 0, capacity, capacity, experts
    )
    routed_rows = routed_rows.reshape(-1, model_width)
    routed_grad = routed_grad.reshape(-1, model_width)
    w_first = gate_weight[0]
    w_third = up_weight[0]
    w_second = down_weight[0]
    contract_last = (((1,), (1,)), ((), ()))
    contract_first = (((0,), (0,)), ((), ()))
    hidden_gate = jnp.dot(routed_rows, w_first, preferred_element_type=jnp.float32)
    hidden_up = jnp.dot(routed_rows, w_third, preferred_element_type=jnp.float32)
    sigma = jax.nn.sigmoid(hidden_gate)
    swish = hidden_gate * sigma
    activ = (swish * hidden_up).astype(jnp.bfloat16)
    grad_second = lax.dot_general(
        activ, routed_grad, contract_first, preferred_element_type=jnp.float32
    ).astype(jnp.bfloat16)
    grad_activ = lax.dot_general(
        routed_grad, w_second, contract_last, preferred_element_type=jnp.float32
    )
    grad_gpre = (grad_activ * hidden_up * sigma * (1.0 + hidden_gate * (1.0 - sigma))).astype(
        jnp.bfloat16
    )
    grad_upre = (grad_activ * swish).astype(jnp.bfloat16)
    grad_first = lax.dot_general(
        routed_rows, grad_gpre, contract_first, preferred_element_type=jnp.float32
    ).astype(jnp.bfloat16)
    grad_third = lax.dot_general(
        routed_rows, grad_upre, contract_first, preferred_element_type=jnp.float32
    ).astype(jnp.bfloat16)
    partial_value = lax.dot_general(
        grad_gpre, w_first, contract_last, preferred_element_type=jnp.float32
    ) + lax.dot_general(grad_upre, w_third, contract_last, preferred_element_type=jnp.float32)
    scattered = sent_and_summed(partial_value.astype(jnp.bfloat16), "tp", 1).astype(jnp.bfloat16)
    home_parts = lax.all_to_all(
        scattered.reshape(experts, capacity, -1), "sp", split_axis=0, concat_axis=0, tiled=True
    )
    home_rows = lax.all_gather(home_parts, "tp", axis=2, tiled=True)
    returned = lax.dot_general(
        full_table,
        home_rows.reshape(-1, model_width),
        contract_first,
        preferred_element_type=jnp.float32,
    )
    mixer_grad = (cotangent.astype(jnp.float32) + returned).astype(jnp.bfloat16)
    normalized_input = saved_normalized.astype(jnp.float32)
    normalized_values = normalized_input * channel_norm_gain[None, :]
    gate_sig = jax.nn.sigmoid(normalized_values)
    act_conv = (normalized_values * gate_sig).astype(jnp.bfloat16)
    grad_proj = sent_and_summed(
        lax.dot_general(
            mixer_grad, act_conv, contract_first, preferred_element_type=jnp.float32
        ).astype(jnp.bfloat16),
        "sp",
        0,
    )
    grad_act = lax.dot_general(
        mixer_grad, proj_weight, contract_last, preferred_element_type=jnp.float32
    )
    norm_output_gradient = (
        grad_act
        * gate_sig
        * (1.0 + normalized_values * (1.0 - gate_sig))
        * channel_norm_gain[None, :]
    )
    reduced_totals = packed_total(
        (
            jnp.sum(norm_output_gradient, axis=1),
            jnp.sum(norm_output_gradient * normalized_input, axis=1),
        ),
        "tp",
    )
    channel_count = saved_normalized.shape[1] * groups
    conv_output_gradient = inverse_deviation[:, None] * (
        norm_output_gradient
        - reduced_totals[0][:, None] / channel_count
        - normalized_input * (reduced_totals[1][:, None] / channel_count)
    )
    reach = taps.shape[0] - 1
    beyond = from_behind(conv_output_gradient[:reach], "sp", -1)
    extended = jnp.concatenate([conv_output_gradient, beyond], axis=0)
    result = jnp.zeros_like(conv_output_gradient)
    for tap_index in range(taps.shape[0]):
        result = result + taps[tap_index][None, :] * extended[tap_index : tap_index + tok_rows]
    return (
        result.astype(jnp.bfloat16),
        grad_proj,
        grad_first[None],
        grad_third[None],
        grad_second[None],
    )


def solution(mesh):
    return jax.shard_map(
        shards,
        mesh=mesh,
        in_specs=(
            P("sp", None),
            P("sp", None),
            P("sp", None),
            P("sp", None),
            P("sp", "tp"),
            P("sp"),
            P("tp"),
            P(None, "tp"),
            P("tp", None),
            P("sp", None, "tp"),
            P("sp", None, "tp"),
            P("sp", "tp", None),
        ),
        out_specs=(
            P("sp", "tp"),
            P("sp", "tp"),
            P("sp", None, "tp"),
            P("sp", None, "tp"),
            P("sp", "tp", None),
        ),
        check_vma=False,
    )
```

profile of v0, /device:TPU:1, one launch (start us, length us, event | category | flops | bytes accessed | tf_op | source)
XLA Modules:
  0.0 256.7 jit_solution(6382690411300353336)
XLA Ops:
  11.6 1.2 fusion.5
  12.9 1.2 fusion.6
  14.5 24.8 %all_to_all.26 = bf16[32,2,2048]{2,1,0:T(2,128)(2,1)S(1)} all-to-all(bf16[32,2,2048]{2,1,0:T(2,128)(2,1)S(1)} %copy.68), channel_id=1, replica_groups=mesh['sp'=32,'tp'=16] {'sp'}, dimensions={0} | all-to-all | bytes 524288 | tf_op jit(solution)/shard_map/all_to_all | solution.py:10
  41.3 42.1 %all-gather.3.cloned.1.call-done = bf16[64,16,2048]{2,0,1:T(8,128)(2,1)} async-done(((bf16[64,1,2048]{2,0,1:T(8,128)(2,1)}), bf16[64,16,2048]{2,0,1:T(8,128)(2,1)}) %all-gather.3.cloned.1.call-update) | async-done | bytes 4194320 | tf_op jit(solution)/shard_map/all_gather | solution.py:26
  83.4 2.7 %fusion.133 = (bf16[32,16,2048]{2,0,1:T(8,128)(2,1)S(1)}, bf16[32,16,2048]{2,0,1:T(8,128)(2,1)S(1)}) fusion(bf16[64,16,2048]{2,0,1:T(8,128)(2,1)} %all-gather.3.cloned.1.call-done), kind=kLoop, calls=%fused_computation.256 | loop fusion | bytes 8388608 | tf_op jit(solution)/shard_map/split | solution.py:26
  86.1 1.2 copy.75
  93.3 55.3 %all_to_all.27 = bf16[16,512,128]{2,1,0:T(8,128)(2,1)} all-to-all(bf16[16,512,128]{2,1,0:T(8,128)(2,1)S(1)} %bitcast.144), channel_id=1, replica_groups=mesh['sp'=32,'tp'=16] {'tp'}, dimensions={0} | all-to-all | bytes 4194304 | tf_op jit(solution)/shard_map/all_to_all | solution.py:37
  148.5 2.6 reduce_sum.72
  151.1 20.5 %all_to_all.28 = bf16[32,16,128]{2,1,0:T(8,128)(2,1)} all-to-all(bf16[32,16,128]{2,1,0:T(8,128)(2,1)} %bitcast.146), channel_id=1, replica_groups=mesh['sp'=32,'tp'=16] {'sp'}, dimensions={0} | all-to-all | bytes 262144 | tf_op jit(solution)/shard_map/all_to_all | solution.py:154
  172.4 1.5 compare_reduce_fusion
  173.9 1.6 slice_bitcast_fusion.29
  175.4 1.6 slice_bitcast_fusion.30
  177.1 3.0 %fusion.3 = bf16[1,128,2048]{2,1,0:T(8,128)(2,1)} fusion(bf16[512,2048]{1,0:T(8,128)(2,1)} %bitcast.143, f32[512,128]{1,0:T(8,128)} %copy-done.5, f32[512,128]{1,0:T(8,128)S(1)} %fusion.12), kind=kOutput, calls=%fused_computation.9 | convolution fusion | flops 269090816 | bytes 3145728 | tf_op jit(solution)/shard_map/dot_general | solution.py:134
  180.1 26.1 %all-gather.5.cloned.1.call-done = bf16[32,16,2048]{2,1,0:T(8,128)(2,1)} async-done(((bf16[32,16,128]{2,1,0:T(8,128)(2,1)}), bf16[32,16,2048]{2,1,0:T(8,128)(2,1)}) %all-gather.5.cloned.1.call-update) | async-done | bytes 2097168 | tf_op jit(solution)/shard_map/all_gather | solution.py:157
  206.2 2.2 fusion
  210.2 5.1 %all-to-all-start.3 = ((f32[16,1,256]{2,1,0:T(1,128)}), f32[16,1,256]{2,1,0:T(1,128)S(1)}, u32[]{:S(2)}, u32[]{:S(2)}) async-start(f32[16,1,256]{2,1,0:T(1,128)} %broadcast_in_dim.22), calls=%async_computation.3 | async-start | bytes 32768 | tf_op jit(solution)/shard_map/all_to_all | solution.py:43
  215.3 2.2 convolution_convert_fusion.3
  217.5 5.2 %all-to-all-done.3 = f32[16,1,256]{2,1,0:T(1,128)S(1)} async-done(((f32[16,1,256]{2,1,0:T(1,128)}), f32[16,1,256]{2,1,0:T(1,128)S(1)}, u32[]{:S(2)}, u32[]{:S(2)}) %all-to-all-start.3) | async-done | bytes 16416 | tf_op jit(solution)/shard_map/all_to_all | solution.py:43
  222.7 9.9 %all-to-all-start.4 = ((bf16[32,64,128]{2,1,0:T(8,128)(2,1)}), bf16[32,64,128]{2,1,0:T(8,128)(2,1)S(1)}, u32[]{:S(2)}, u32[]{:S(2)}) async-start(bf16[32,64,128]{2,1,0:T(8,128)(2,1)} %bitcast.42), calls=%async_computation.4 | async-start | bytes 1048576 | tf_op jit(solution)/shard_map/all_to_all | solution.py:37
  232.6 1.6 fusion.2
  234.6 1.3 collective-permute-start
  235.9 1.6 fusion.1
  237.5 2.3 collective-permute-done
  240.9 8.3 %all-to-all-done.4 = bf16[32,64,128]{2,1,0:T(8,128)(2,1)S(1)} async-done(((bf16[32,64,128]{2,1,0:T(8,128)(2,1)}), bf16[32,64,128]{2,1,0:T(8,128)(2,1)S(1)}, u32[]{:S(2)}, u32[]{:S(2)}) %all-to-all-start.4) | async-done | bytes 524320 | tf_op jit(solution)/shard_map/all_to_all | solution.py:37
  (125 shorter events, 17.0 us)
Async XLA Ops:
  7.2 81.3 %copy-start = (bf16[1,2048,128]{2,1,0:T(8,128)(2,1)S(1)}, bf16[1,2048,128]{2,1,0:T(8,128)(2,1)}, u32[]{:S(2)}) copy-start(bf16[1,2048,128]{2,1,0:T(8,128)(2,1)} %param.21) | copy-start | bytes 1572868
  7.2 76.2 %all-gather.3.cloned.1.call-start = ((), (), s32[]{:S(2)}) async-start(), calls=%async_computation.5 | async-start | bytes 4456448 | tf_op jit(solution)/shard_map/all_gather | solution.py:26
  41.2 165.0 %all-gather.5.cloned.1.call-start = ((), (), s32[]{:S(2)}) async-start(), calls=%async_computation.6 | async-start | bytes 2228224 | tf_op jit(solution)/shard_map/all_gather | solution.py:157
  151.1 55.1 %copy-start.2 = (bf16[128,2048]{1,0:T(8,128)(2,1)S(1)}, bf16[128,2048]{1,0:T(8,128)(2,1)}, u32[]{:S(2)}) copy-start(bf16[128,2048]{1,0:T(8,128)(2,1)} %param.12) | copy-start | bytes 1572868
  180.1 29.1 %copy-start.8 = (bf16[128,128]{1,0:T(8,128)(2,1)S(1)}, bf16[128,128]{1,0:T(8,128)(2,1)}, u32[]{:S(2)}) copy-start(bf16[128,128]{1,0:T(8,128)(2,1)} %param.16) | copy-start | bytes 98308
  180.1 29.1 %copy-start.37 = (f32[128]{0:T(128)S(1)}, f32[128]{0:T(128)}, u32[]{:S(2)}) copy-start(f32[128]{0:T(128)} %param.18) | copy-start | bytes 1540
  209.2 23.4 %copy-start.7 = (bf16[512,128]{1,0:T(8,128)(2,1)S(1)}, bf16[512,128]{1,0:T(8,128)(2,1)}, u32[]{:S(2)}) copy-start(bf16[512,128]{1,0:T(8,128)(2,1)} %copy-done.6) | copy-start | bytes 393220
  210.2 12.5 %all-to-all-start.3 = ((f32[16,1,256]{2,1,0:T(1,128)}), f32[16,1,256]{2,1,0:T(1,128)S(1)}, u32[]{:S(2)}, u32[]{:S(2)}) async-start(f32[16,1,256]{2,1,0:T(1,128)} %broadcast_in_dim.22), calls=%async_computation.3 | async-start | bytes 32768 | tf_op jit(solution)/shard_map/all_to_all | solution.py:43
  222.7 26.5 %all-to-all-start.4 = ((bf16[32,64,128]{2,1,0:T(8,128)(2,1)}), bf16[32,64,128]{2,1,0:T(8,128)(2,1)S(1)}, u32[]{:S(2)}, u32[]{:S(2)}) async-start(bf16[32,64,128]{2,1,0:T(8,128)(2,1)} %bitcast.42), calls=%async_computation.4 | async-start | bytes 1048576 | tf_op jit(solution)/shard_map/all_to_all | solution.py:37
  234.3 5.4 %copy-start.10 = (f32[128]{0:T(128)S(1)}, f32[128]{0:T(128)}, u32[]{:S(2)}) copy-start(f32[128]{0:T(128)} %get-tuple-element.36) | copy-start | bytes 1540
  234.3 5.4 %copy-start.11 = (f32[128]{0:T(128)S(1)}, f32[128]{0:T(128)}, u32[]{:S(2)}) copy-start(f32[128]{0:T(128)} %get-tuple-element.37) | copy-start | bytes 1540
  234.4 5.4 %copy-start.12 = (f32[128]{0:T(128)S(1)}, f32[128]{0:T(128)}, u32[]{:S(2)}) copy-start(f32[128]{0:T(128)} %get-tuple-element.38) | copy-start | bytes 1540
  234.4 5.4 %copy-start.13 = (f32[128]{0:T(128)S(1)}, f32[128]{0:T(128)}, u32[]{:S(2)}) copy-start(f32[128]{0:T(128)} %get-tuple-element.39) | copy-start | bytes 1540
  234.4 5.4 %copy-start.14 = (f32[128]{0:T(128)S(1)}, f32[128]{0:T(128)}, u32[]{:S(2)}) copy-start(f32[128]{0:T(128)} %get-tuple-element.40) | copy-start | bytes 1540
  234.4 5.4 %copy-start.15 = (f32[128]{0:T(128)S(1)}, f32[128]{0:T(128)}, u32[]{:S(2)}) copy-start(f32[128]{0:T(128)} %get-tuple-element.41) | copy-start | bytes 1540
  234.4 5.4 %copy-start.16 = (f32[128]{0:T(128)S(1)}, f32[128]{0:T(128)}, u32[]{:S(2)}) copy-start(f32[128]{0:T(128)} %get-tuple-element.42) | copy-start | bytes 1540
  234.4 5.4 %copy-start.17 = (f32[128]{0:T(128)S(1)}, f32[128]{0:T(128)}, u32[]{:S(2)}) copy-start(f32[128]{0:T(128)} %get-tuple-element.43) | copy-start | bytes 1540
  234.4 5.4 %copy-start.18 = (f32[128]{0:T(128)S(1)}, f32[128]{0:T(128)}, u32[]{:S(2)}) copy-start(f32[128]{0:T(128)} %get-tuple-element.13) | copy-start | bytes 1540
  234.4 5.4 %copy-start.19 = (f32[128]{0:T(128)S(1)}, f32[128]{0:T(128)}, u32[]{:S(2)}) copy-start(f32[128]{0:T(128)} %get-tuple-element.14) | copy-start | bytes 1540
  234.4 5.4 %copy-start.20 = (f32[128]{0:T(128)S(1)}, f32[128]{0:T(128)}, u32[]{:S(2)}) copy-start(f32[128]{0:T(128)} %get-tuple-element.15) | copy-start | bytes 1540
  234.4 5.4 %copy-start.21 = (f32[128]{0:T(128)S(1)}, f32[128]{0:T(128)}, u32[]{:S(2)}) copy-start(f32[128]{0:T(128)} %get-tuple-element.16) | copy-start | bytes 1540
  234.5 5.4 %copy-start.22 = (f32[128]{0:T(128)S(1)}, f32[128]{0:T(128)}, u32[]{:S(2)}) copy-start(f32[128]{0:T(128)} %get-tuple-element.17) | copy-start | bytes 1540
  234.5 5.4 %copy-start.23 = (f32[128]{0:T(128)S(1)}, f32[128]{0:T(128)}, u32[]{:S(2)}) copy-start(f32[128]{0:T(128)} %get-tuple-element.18) | copy-start | bytes 1540
  234.6 5.2 %collective-permute-start = (f32[30,128]{1,0:T(8,128)S(1)}, f32[30,128]{1,0:T(8,128)S(1)}, u32[]{:S(2)}, u32[]{:S(2)}) collective-permute-start(f32[30,128]{1,0:T(8,128)S(1)} %slice.275), channel_id=1, source_target_pairs={{16,0},{32,16},{48,32},{64,48},{80,64},{96,80},{112,96},{128,112},... | collective-permute-start | bytes 46088 | tf_op jit(solution)/shard_map/ppermute | solution.py:64
  (22 other events, 83.3 us)
Sparse Core Ops, SparseCore 0:
  41.3 42.0 all-gather.2
  171.8 34.3 all-gather.4
where the time goes:
time: 258 us; the launch traced here: 257 us
  blocking collectives  101 us (39%)
  waiting for transfers between devices  84 us (33%)
  matrix products  16.9 us (7%)
  starting transfers between devices  16.4 us (6%)
  local copies, waits for them, and re-layouts  15.1 us (6%)
  between operations  14.8 us (6%)
  other arithmetic  8.92 us (3%)
    all_to_all x1, blocking collectives, sent_and_summed(): lax.all_to_all(pieces, axis, split_axis=0, concat_axis=0, tiled=True)  55.3 us
    all_gather x1, waiting for transfers between devices, side_by_side(): lax.all_gather(both, axis, axis=dim, tiled=True)  42.1 us
    all_gather x1, waiting for transfers between devices, shards(): home_rows = lax.all_gather(home_parts, 'tp', axis=2, tiled=True)  26.1 us
    all_to_all x1, blocking collectives, sent_together(): lax.all_to_all(both, axis, split_axis=split_dim, concat_axis=concat_dim,...  24.8 us
    all_to_all x1, blocking collectives, shards(): lax.all_to_all(scattered.reshape(experts, capacity, -1), 'sp', split_axis...  20.5 us
    all_to_all x1, starting transfers between devices, sent_and_summed(): lax.all_to_all(pieces, axis, split_axis=0, concat_axis=0, tiled=True)  9.9 us
    all_to_all x1, waiting for transfers between devices, sent_and_summed(): lax.all_to_all(pieces, axis, split_axis=0, concat_axis=0, tiled=True)  8.31 us
    unnamed x85, local copies, waits for them, and re-layouts  5.2 us
  transfers between devices with their start and end apart: 5, of which 5 were waited for; matrix products, arithmetic and copies ran while one was open for 6% of the time, Pallas kernels for 0%

commit v1 on v0

--- a/solution.py
+++ b/solution.py
@@ -154,7 +154,9 @@
     home_parts = lax.all_to_all(
         scattered.reshape(experts, capacity, -1), "sp", split_axis=0, concat_axis=0, tiled=True
     )
-    home_rows = lax.all_gather(home_parts, "tp", axis=2, tiled=True)
+    home_rows = jnp.concatenate(
+        lax.all_to_all(jnp.stack([home_parts] * lax.axis_size("tp")), "tp", 0, 0), axis=2
+    )
     returned = lax.dot_general(
         full_table,
         home_rows.reshape(-1, model_width),

time: 258 us -> 273 us (1.058)
  waiting for transfers between devices: 84 us -> 101 us
  local copies, waits for them, and re-layouts: 15.1 us -> 17.9 us
    all_to_all x0 -> x1, waiting for transfers between devices: none -> 43.5 us  [shards(): lax.all_to_all(jnp.stack([home_parts] * lax.axis_size('tp')), 'tp', 0, 0)]
    all_gather x1 -> x0, waiting for transfers between devices: 26.1 us -> none  [shards(): home_rows = lax.all_gather(home_parts, 'tp', axis=2, tiled=True)]
    all_to_all x1, starting transfers between devices: 9.9 us -> 3.89 us  [sent_and_summed(): lax.all_to_all(pieces, axis, split_axis=0, concat_axis=0, tiled=True)]
    all_to_all x0 -> x1, starting transfers between devices: none -> 4.65 us  [shards(): lax.all_to_all(jnp.stack([home_parts] * lax.axis_size('tp')), 'tp', 0, 0)]
    reshape x0 -> x1, local copies, waits for them, and re-layouts: none -> 4.08 us  [shards(): jnp.concatenate(lax.all_to_all(jnp.stack([home_parts] * lax.axis_size('tp...]
  transfers between devices with their start and end apart: 5 -> 5, of which waited for: 5 -> 5; matrix products, arithmetic and copies ran while one was open for 6% -> 4% of each run, Pallas kernels for 0% -> 0%
where the time goes in v1:
time: 273 us; the launch traced here: 272 us
  waiting for transfers between devices  101 us (37%)
  blocking collectives  100 us (37%)
  local copies, waits for them, and re-layouts  17.9 us (7%)
  starting transfers between devices  15.3 us (6%)
  matrix products  15.1 us (6%)
  between operations  14.7 us (5%)
  other arithmetic  7.55 us (3%)
    all_to_all x1, blocking collectives, sent_and_summed(): lax.all_to_all(pieces, axis, split_axis=0, concat_axis=0, tiled=True)  55.3 us
    all_to_all x1, waiting for transfers between devices, shards(): lax.all_to_all(jnp.stack([home_parts] * lax.axis_size('tp')), 'tp', 0, 0)  43.5 us
    all_gather x1, waiting for transfers between devices, side_by_side(): lax.all_gather(both, axis, axis=dim, tiled=True)  42.2 us
    all_to_all x1, blocking collectives, sent_together(): lax.all_to_all(both, axis, split_axis=split_dim, concat_axis=concat_dim,...  24.8 us
    all_to_all x1, blocking collectives, shards(): lax.all_to_all(scattered.reshape(experts, capacity, -1), 'sp', split_axis...  20.1 us
    all_to_all x1, waiting for transfers between devices, sent_and_summed(): lax.all_to_all(pieces, axis, split_axis=0, concat_axis=0, tiled=True)  7.87 us
  transfers between devices with their start and end apart: 5, of which 5 were waited for; matrix products, arithmetic and copies ran while one was open for 4% of the time, Pallas kernels for 0%

profile of v1, /device:TPU:1, one launch (start us, length us, event | category | flops | bytes accessed | tf_op | source)
XLA Modules:
  0.0 271.7 jit_solution(6538250690136339697)
XLA Ops:
  11.2 1.2 fusion.5
  12.4 1.2 fusion.6
  14.0 24.8 %all_to_all.31 = bf16[32,2,2048]{2,1,0:T(2,128)(2,1)S(1)} all-to-all(bf16[32,2,2048]{2,1,0:T(2,128)(2,1)S(1)} %copy.71), channel_id=1, replica_groups=mesh['sp'=32,'tp'=16] {'sp'}, dimensions={0} | all-to-all | bytes 524288 | tf_op jit(solution)/shard_map/all_to_all | solution.py:10
  40.7 42.2 %all-gather.2.cloned.1.call-done = bf16[64,16,2048]{2,0,1:T(8,128)(2,1)} async-done(((bf16[64,1,2048]{2,0,1:T(8,128)(2,1)}), bf16[64,16,2048]{2,0,1:T(8,128)(2,1)}) %all-gather.2.cloned.1.call-update) | async-done | bytes 4194320 | tf_op jit(solution)/shard_map/all_gather | solution.py:26
  82.9 2.7 %fusion.135 = (bf16[32,16,2048]{2,0,1:T(8,128)(2,1)S(1)}, bf16[32,16,2048]{2,0,1:T(8,128)(2,1)S(1)}) fusion(bf16[64,16,2048]{2,0,1:T(8,128)(2,1)} %all-gather.2.cloned.1.call-done), kind=kLoop, calls=%fused_computation.258 | loop fusion | bytes 8388608 | tf_op jit(solution)/shard_map/split | solution.py:26
  85.6 1.2 copy.79
  86.8 1.2 copy.80
  92.8 55.3 %all_to_all.32 = bf16[16,512,128]{2,1,0:T(8,128)(2,1)} all-to-all(bf16[16,512,128]{2,1,0:T(8,128)(2,1)S(1)} %bitcast.148), channel_id=1, replica_groups=mesh['sp'=32,'tp'=16] {'tp'}, dimensions={0} | all-to-all | bytes 4194304 | tf_op jit(solution)/shard_map/all_to_all | solution.py:37
  148.0 1.9 reduce_sum.72
  149.9 20.1 %all_to_all.33 = bf16[32,16,128]{2,1,0:T(8,128)(2,1)S(1)} all-to-all(bf16[32,16,128]{2,1,0:T(8,128)(2,1)S(1)} %bitcast.150), channel_id=1, replica_groups=mesh['sp'=32,'tp'=16] {'sp'}, dimensions={0} | all-to-all | bytes 262144 | tf_op jit(solution)/shard_map/all_to_all | solution.py:154
  170.0 1.7 stack.2
  171.7 4.7 %all-to-all-start.3 = ((bf16[16,32,16,128]{3,2,1,0:T(8,128)(2,1)}), bf16[16,32,16,128]{3,2,1,0:T(8,128)(2,1)}, u32[]{:S(2)}, u32[]{:S(2)}) async-start(bf16[16,32,16,128]{3,2,1,0:T(8,128)(2,1)} %stack.2), calls=%async_computation.3 | async-start | bytes 4194304 | tf_op jit(solution)/shard_map/all_to_all | solution.py:158
  178.0 2.9 %fusion.3 = bf16[1,128,2048]{2,1,0:T(8,128)(2,1)} fusion(bf16[512,2048]{1,0:T(8,128)(2,1)} %bitcast.147, f32[512,128]{1,0:T(8,128)S(1)} %fusion.17, f32[512,128]{1,0:T(8,128)S(1)} %fusion.14), kind=kOutput, calls=%fused_computation.9 | convolution fusion | flops 269090816 | bytes 3145728 | tf_op jit(solution)/shard_map/dot_general | solution.py:134
  180.9 43.5 %all-to-all-done.3 = bf16[16,32,16,128]{3,2,1,0:T(8,128)(2,1)} async-done(((bf16[16,32,16,128]{3,2,1,0:T(8,128)(2,1)}), bf16[16,32,16,128]{3,2,1,0:T(8,128)(2,1)}, u32[]{:S(2)}, u32[]{:S(2)}) %all-to-all-start.3) | async-done | bytes 2097184 | tf_op jit(solution)/shard_map/all_to_all | solution.py:158
  224.4 4.1 %copy.76 = bf16[32,16,16,128]{3,2,1,0:T(8,128)(2,1)S(1)} copy(bf16[32,16,16,128]{3,1,0,2:T(8,128)(2,1)} %bitcast.11) | data formatting | bytes 4194304 | tf_op jit(solution)/shard_map/reshape | solution.py:157
  230.8 5.5 %all-to-all-start.4 = ((f32[16,1,256]{2,1,0:T(1,128)}), f32[16,1,256]{2,1,0:T(1,128)S(1)}, u32[]{:S(2)}, u32[]{:S(2)}) async-start(f32[16,1,256]{2,1,0:T(1,128)} %broadcast_in_dim.22), calls=%async_computation.4 | async-start | bytes 32768 | tf_op jit(solution)/shard_map/all_to_all | solution.py:43
  236.3 2.2 convolution_convert_fusion.3
  238.5 5.2 %all-to-all-done.4 = f32[16,1,256]{2,1,0:T(1,128)S(1)} async-done(((f32[16,1,256]{2,1,0:T(1,128)}), f32[16,1,256]{2,1,0:T(1,128)S(1)}, u32[]{:S(2)}, u32[]{:S(2)}) %all-to-all-start.4) | async-done | bytes 16416 | tf_op jit(solution)/shard_map/all_to_all | solution.py:43
  243.6 3.9 %all-to-all-start.5 = ((bf16[32,64,128]{2,1,0:T(8,128)(2,1)}), bf16[32,64,128]{2,1,0:T(8,128)(2,1)S(1)}, u32[]{:S(2)}, u32[]{:S(2)}) async-start(bf16[32,64,128]{2,1,0:T(8,128)(2,1)} %bitcast.42), calls=%async_computation.5 | async-start | bytes 1048576 | tf_op jit(solution)/shard_map/all_to_all | solution.py:37
  247.5 1.6 fusion.2
  250.2 1.3 collective-permute-start
  251.5 1.6 fusion.1
  253.0 2.2 collective-permute-done
  256.3 7.9 %all-to-all-done.5 = bf16[32,64,128]{2,1,0:T(8,128)(2,1)S(1)} async-done(((bf16[32,64,128]{2,1,0:T(8,128)(2,1)}), bf16[32,64,128]{2,1,0:T(8,128)(2,1)S(1)}, u32[]{:S(2)}, u32[]{:S(2)}) %all-to-all-start.5) | async-done | bytes 524320 | tf_op jit(solution)/shard_map/all_to_all | solution.py:37
  (110 shorter events, 17.2 us)
Async XLA Ops:
  7.2 80.8 %copy-start = (bf16[1,2048,128]{2,1,0:T(8,128)(2,1)S(1)}, bf16[1,2048,128]{2,1,0:T(8,128)(2,1)}, u32[]{:S(2)}) copy-start(bf16[1,2048,128]{2,1,0:T(8,128)(2,1)} %param.21) | copy-start | bytes 1572868
  7.2 75.7 %all-gather.2.cloned.1.call-start = ((), (), s32[]{:S(2)}) async-start(), calls=%async_computation.6 | async-start | bytes 4456448 | tf_op jit(solution)/shard_map/all_gather | solution.py:26
  171.7 52.6 %all-to-all-start.3 = ((bf16[16,32,16,128]{3,2,1,0:T(8,128)(2,1)}), bf16[16,32,16,128]{3,2,1,0:T(8,128)(2,1)}, u32[]{:S(2)}, u32[]{:S(2)}) async-start(bf16[16,32,16,128]{3,2,1,0:T(8,128)(2,1)} %stack.2), calls=%async_computation.3 | async-start | bytes 4194304 | tf_op jit(solution)/shard_map/all_to_all | solution.py:158
  230.8 12.8 %all-to-all-start.4 = ((f32[16,1,256]{2,1,0:T(1,128)}), f32[16,1,256]{2,1,0:T(1,128)S(1)}, u32[]{:S(2)}, u32[]{:S(2)}) async-start(f32[16,1,256]{2,1,0:T(1,128)} %broadcast_in_dim.22), calls=%async_computation.4 | async-start | bytes 32768 | tf_op jit(solution)/shard_map/all_to_all | solution.py:43
  243.6 20.6 %all-to-all-start.5 = ((bf16[32,64,128]{2,1,0:T(8,128)(2,1)}), bf16[32,64,128]{2,1,0:T(8,128)(2,1)S(1)}, u32[]{:S(2)}, u32[]{:S(2)}) async-start(bf16[32,64,128]{2,1,0:T(8,128)(2,1)} %bitcast.42), calls=%async_computation.5 | async-start | bytes 1048576 | tf_op jit(solution)/shard_map/all_to_all | solution.py:37
  249.9 5.3 %copy-start.7 = (f32[128]{0:T(128)S(1)}, f32[128]{0:T(128)}, u32[]{:S(2)}) copy-start(f32[128]{0:T(128)} %get-tuple-element.40) | copy-start | bytes 1540
  249.9 5.3 %copy-start.8 = (f32[128]{0:T(128)S(1)}, f32[128]{0:T(128)}, u32[]{:S(2)}) copy-start(f32[128]{0:T(128)} %get-tuple-element.41) | copy-start | bytes 1540
  250.0 5.3 %copy-start.9 = (f32[128]{0:T(128)S(1)}, f32[128]{0:T(128)}, u32[]{:S(2)}) copy-start(f32[128]{0:T(128)} %get-tuple-element.42) | copy-start | bytes 1540
  250.0 5.3 %copy-start.10 = (f32[128]{0:T(128)S(1)}, f32[128]{0:T(128)}, u32[]{:S(2)}) copy-start(f32[128]{0:T(128)} %get-tuple-element.43) | copy-start | bytes 1540
  250.0 5.3 %copy-start.11 = (f32[128]{0:T(128)S(1)}, f32[128]{0:T(128)}, u32[]{:S(2)}) copy-start(f32[128]{0:T(128)} %get-tuple-element.13) | copy-start | bytes 1540
  250.0 5.3 %copy-start.12 = (f32[128]{0:T(128)S(1)}, f32[128]{0:T(128)}, u32[]{:S(2)}) copy-start(f32[128]{0:T(128)} %get-tuple-element.14) | copy-start | bytes 1540
  250.0 5.3 %copy-start.13 = (f32[128]{0:T(128)S(1)}, f32[128]{0:T(128)}, u32[]{:S(2)}) copy-start(f32[128]{0:T(128)} %get-tuple-element.15) | copy-start | bytes 1540
  250.0 5.3 %copy-start.14 = (f32[128]{0:T(128)S(1)}, f32[128]{0:T(128)}, u32[]{:S(2)}) copy-start(f32[128]{0:T(128)} %get-tuple-element.16) | copy-start | bytes 1540
  250.0 5.3 %copy-start.15 = (f32[128]{0:T(128)S(1)}, f32[128]{0:T(128)}, u32[]{:S(2)}) copy-start(f32[128]{0:T(128)} %get-tuple-element.17) | copy-start | bytes 1540
  250.0 5.3 %copy-start.16 = (f32[128]{0:T(128)S(1)}, f32[128]{0:T(128)}, u32[]{:S(2)}) copy-start(f32[128]{0:T(128)} %get-tuple-element.18) | copy-start | bytes 1540
  250.0 5.3 %copy-start.17 = (f32[128]{0:T(128)S(1)}, f32[128]{0:T(128)}, u32[]{:S(2)}) copy-start(f32[128]{0:T(128)} %get-tuple-element.19) | copy-start | bytes 1540
  250.0 5.3 %copy-start.18 = (f32[128]{0:T(128)S(1)}, f32[128]{0:T(128)}, u32[]{:S(2)}) copy-start(f32[128]{0:T(128)} %get-tuple-element.20) | copy-start | bytes 1540
  250.1 5.3 %copy-start.19 = (f32[128]{0:T(128)S(1)}, f32[128]{0:T(128)}, u32[]{:S(2)}) copy-start(f32[128]{0:T(128)} %get-tuple-element.21) | copy-start | bytes 1540
  250.1 5.3 %copy-start.20 = (f32[128]{0:T(128)S(1)}, f32[128]{0:T(128)}, u32[]{:S(2)}) copy-start(f32[128]{0:T(128)} %get-tuple-element.22) | copy-start | bytes 1540
  250.1 5.3 %copy-start.21 = (f32[128]{0:T(128)S(1)}, f32[128]{0:T(128)}, u32[]{:S(2)}) copy-start(f32[128]{0:T(128)} %get-tuple-element.23) | copy-start | bytes 1540
  250.1 5.3 %copy-start.22 = (f32[128]{0:T(128)S(1)}, f32[128]{0:T(128)}, u32[]{:S(2)}) copy-start(f32[128]{0:T(128)} %get-tuple-element.24) | copy-start | bytes 1540
  250.1 5.3 %copy-start.23 = (f32[128]{0:T(128)S(1)}, f32[128]{0:T(128)}, u32[]{:S(2)}) copy-start(f32[128]{0:T(128)} %get-tuple-element.25) | copy-start | bytes 1540
  250.1 5.3 %copy-start.24 = (f32[128]{0:T(128)S(1)}, f32[128]{0:T(128)}, u32[]{:S(2)}) copy-start(f32[128]{0:T(128)} %get-tuple-element.26) | copy-start | bytes 1540
  250.2 5.1 %collective-permute-start = (f32[30,128]{1,0:T(8,128)S(1)}, f32[30,128]{1,0:T(8,128)S(1)}, u32[]{:S(2)}, u32[]{:S(2)}) collective-permute-start(f32[30,128]{1,0:T(8,128)S(1)} %slice.275), channel_id=1, source_target_pairs={{16,0},{32,16},{48,32},{64,48},{80,64},{96,80},{112,96},{128,112},... | collective-permute-start | bytes 46088 | tf_op jit(solution)/shard_map/ppermute | solution.py:64
  (14 other events, 45.5 us)
Sparse Core Ops, SparseCore 0:
  40.8 42.0 all-gather.1
